TPU v7x, 32 devices: a whole 2x2x4 slice. The times are simulated.
32 devices in a mesh: grp: 2 (over x), ep: 16 (over z, y, core).
Axes of the slice: x: 2, y: 2, z: 4, core: 2. Of those that a mesh axis runs over, the one named last changes fastest.
Arguments:
- tokens: bfloat16 [128, 2048], P(('grp', 'ep')), parts along dimension 0, may hold values from -30 to 30
- state: float32 [128, 16, 128, 128], P(('grp', 'ep')), parts along dimension 0, may hold values from -6 to 6
- route_ids: int32 [128, 2], P(('grp', 'ep')), parts along dimension 0, may hold values from 0 to 3, all different within a row; in each aligned block of 4 rows (0 to 3, 4 to 7, ...) at most 3 rows name the same one
- route_weights: bfloat16 [128, 2], P(('grp', 'ep')), parts along dimension 0, may hold values from 0.099609375 to 1
- norm_mix: float32 [2048], replicated, may hold values from 0.1 to 1.9
- w_query: bfloat16 [2048, 2048], P(None, 'ep'), may hold values from -0.125 to 0.125
- w_forget: bfloat16 [2048, 2048], P(None, 'ep'), may hold values from -0.125 to 0.125
- w_input: bfloat16 [2048, 2048], P(None, 'ep'), may hold values from -0.125 to 0.125
- w_gate: bfloat16 [2048, 2048], P(None, 'ep'), may hold values from -0.125 to 0.125
- lower_bound: float32 [2048], replicated, may hold values from 0.05 to 0.9
- head_gain: float32 [128], replicated, may hold values from 0.1 to 1.9
- w_out: bfloat16 [2048, 2048], P(None, 'ep'), may hold values from -0.125 to 0.125
- norm_ffn: float32 [2048], replicated, may hold values from 0.1 to 1.9
- expert_gate: bfloat16 [2048, 28672], P(None, 'ep'), may hold values from -0.125 to 0.125
- expert_up: bfloat16 [2048, 28672], P(None, 'ep'), may hold values from -0.125 to 0.125
- expert_down: bfloat16 [28672, 2048], P('ep'), may hold values from -0.0625 to 0.0625
Outputs:
- layer_out: bfloat16 [128, 2048], P(('grp', 'ep')), parts along dimension 0
- new_state: float32 [128, 16, 128, 128], P(('grp', 'ep')), parts along dimension 0
There are 2 independent parts, one for each index of `grp`. A program takes and returns all parts, laid end to end along the dimension named above; an argument that names none is the same for every part. Nothing has to cross between parts.
Inputs may be any that keep to these rules, and one draw needn't show every extreme that they name: `route_ids`: each row names 2 different experts; the rows of one device name no expert more than 3 times, and some device names one exactly 3 times.
All inputs are finite; a program needn't handle non-finite values.
Results may differ from a plain program's by a relative error of at most 0.008.
Values may be sent and summed in bfloat16 or wider, within the bound.
No kernel may reach another device: no remote copies, remote signals or barrier semaphores. Data moves between devices by JAX's collectives and lax.ppermute only.
A program may use at most 64 MiB of HBM per device.

v0:
```python
import jax
import jax.numpy as jnp
from jax import lax
from jax.sharding import PartitionSpec as P

FF = 7168
EXPERTS = 4
CAP = 3
epsilon = 1e-06


def rms_scale(values, gain):
    return values * lax.rsqrt(jnp.mean(values * values, axis=-1, keepdims=True) + epsilon) * gain


def mixer_state(projected, state, lower_bound, head_gain):
    query_raw = projected[0].astype(jnp.float32)
    forget_raw = projected[1].astype(jnp.float32)
    input_raw = projected[2].astype(jnp.float32)
    gate_raw = projected[3].astype(jnp.float32)
    seq_rows = state.shape[0]
    heads = state.shape[1]
    head_dim = state.shape[2]
    head_shape = (seq_rows, heads, head_dim)
    log_forget = jnp.logaddexp(
        jnp.log(lower_bound), jnp.log1p(-lower_bound) + jax.nn.log_sigmoid(forget_raw)
    )
    key_vec = (1.0 - lower_bound) * jax.nn.sigmoid(-forget_raw)
    query_vec = jax.nn.silu(query_raw) * head_dim ** (-0.5)
    new_state = (
        jnp.exp(log_forget).reshape(head_shape)[..., None] * state
        + key_vec.reshape(head_shape)[..., None] * input_raw.reshape(head_shape)[:, :, None, :]
    )
    read_out = jnp.einsum(
        "thk,thkv->thv", query_vec.reshape(head_shape), new_state, precision=lax.Precision.HIGHEST
    )
    mixed = rms_scale(read_out, head_gain) * jax.nn.silu(gate_raw.reshape(head_shape))
    return (mixed.reshape(seq_rows, heads * head_dim).astype(jnp.bfloat16), new_state)


def local(
    tokens,
    state,
    route_ids,
    route_weights,
    norm_mix,
    w_query,
    w_forget,
    w_input,
    w_gate,
    lower_bound,
    head_gain,
    w_out,
    norm_ffn,
    expert_gate,
    expert_up,
    expert_down,
):
    model_width = tokens.shape[1]
    expert_group = FF // expert_gate.shape[1]
    all_tokens, all_ids, all_weights = (
        lax.all_gather(tokens, "ep", axis=0, tiled=True),
        lax.all_gather(route_ids, "ep", axis=0, tiled=True),
        lax.all_gather(route_weights, "ep", axis=0, tiled=True),
    )
    normed = rms_scale(all_tokens.astype(jnp.float32), norm_mix).astype(jnp.bfloat16)
    projected = jnp.stack(
        [
            jnp.dot(normed, weight, preferred_element_type=jnp.float32).astype(jnp.bfloat16)
            for weight in (w_query, w_forget, w_input, w_gate)
        ]
    )
    owned = lax.all_to_all(projected, "ep", split_axis=1, concat_axis=2, tiled=True)
    mixed, new_state = mixer_state(owned, state, lower_bound, head_gain)
    mixer_cols = jnp.dot(
        lax.all_gather(mixed, "ep", axis=0, tiled=True), w_out, preferred_element_type=jnp.float32
    ).astype(jnp.bfloat16)
    mixer_rows = lax.all_to_all(mixer_cols, "ep", split_axis=0, concat_axis=1, tiled=True)
    middle = tokens.astype(jnp.float32) + mixer_rows.astype(jnp.float32)
    normed_two = rms_scale(middle, norm_ffn).astype(jnp.bfloat16)
    matches = (route_ids[:, :, None] == jnp.arange(EXPERTS, dtype=jnp.int32)[None, None, :]).astype(
        jnp.int32
    )
    hit_mask = jnp.sum(matches, axis=1)
    combined = jnp.sum(
        route_weights.astype(jnp.float32)[:, :, None] * matches.astype(jnp.float32), axis=1
    )
    slot_rank = jnp.cumsum(hit_mask, axis=0) - hit_mask
    slot_ids = jnp.arange(CAP, dtype=jnp.int32)
    placing = (
        (slot_rank.T[:, None, :] == slot_ids[None, :, None]) & (hit_mask.T[:, None, :] > 0)
    ).astype(jnp.float32)
    outgoing = jnp.einsum(
        "ect,td->ecd", placing.astype(jnp.bfloat16), normed_two, preferred_element_type=jnp.float32
    ).astype(jnp.bfloat16)
    outgoing = jnp.repeat(outgoing, expert_group, axis=0)
    arrived = lax.all_to_all(outgoing, "ep", split_axis=0, concat_axis=0, tiled=True)
    gate_act = jnp.einsum("scd,df->scf", arrived, expert_gate, preferred_element_type=jnp.float32)
    up_act = jnp.einsum("scd,df->scf", arrived, expert_up, preferred_element_type=jnp.float32)
    hidden = (jax.nn.silu(gate_act) * up_act).astype(jnp.bfloat16)
    partial_rows = jnp.einsum(
        "scf,fd->scd", hidden, expert_down, preferred_element_type=jnp.float32
    )
    returned = lax.all_to_all(
        partial_rows.astype(jnp.bfloat16), "ep", split_axis=0, concat_axis=0, tiled=True
    ).astype(partial_rows.dtype)
    summed = jnp.sum(
        returned.reshape(EXPERTS, expert_group, returned.shape[1], model_width), axis=1
    )
    expert_total = jnp.einsum(
        "ect,ecd->td", placing * combined.T[:, None, :], summed, precision=lax.Precision.HIGHEST
    )
    layer_out = (middle + expert_total).astype(jnp.bfloat16)
    return (layer_out, new_state)


def solution(mesh):
    return jax.shard_map(
        local,
        mesh=mesh,
        in_specs=(
            P(("grp", "ep"), None),
            P(("grp", "ep"), None, None, None),
            P(("grp", "ep"), None),
            P(("grp", "ep"), None),
            P(),
            P(None, "ep"),
            P(None, "ep"),
            P(None, "ep"),
            P(None, "ep"),
            P(),
            P(),
            P(None, "ep"),
            P(),
            P(None, "ep"),
            P(None, "ep"),
            P("ep", None),
        ),
        out_specs=(P(("grp", "ep"), None), P(("grp", "ep"), None, None, None)),
        check_vma=False,
    )
```

profile of v0, /device:TPU:0, one launch (start us, length us, event | category | flops | bytes accessed | tf_op | source)
XLA Modules:
  0.0 121.8 jit_solution(15939425539012757206)
XLA Ops:
  0.6 0.0 copy-start
  0.6 24.2 %all-gather = bf16[16,4,2048]{2,1,0:T(4,128)(2,1)S(1)} all-gather(bf16[1,4,2048]{2,1,0:T(4,128)(2,1)} %bitcast.138), channel_id=1, replica_groups=mesh['grp'=2,'ep'=16] {'ep'}, dimensions={0}, use_global_device_ids=true | all-gather | bytes 278528 | tf_op jit(solution)/shard_map/all_gather | solution.py:62
  24.9 0.1 multiply_reduce_fusion
  25.0 0.8 multiply_convert_fusion
  25.9 0.0 copy-done
  25.9 0.2 fusion.17
  26.1 1.3 %fusion.18 = bf16[1,64,128]{2,1,0:T(8,128)(2,1)S(1)} fusion(bf16[64,2048]{1,0:T(8,128)(2,1)S(1)} %multiply_convert_fusion, bf16[2048,128]{1,0:T(8,128)(2,1)} %param.22), kind=kOutput, calls=%fused_computation.20 | convolution fusion | flops 33562624 | bytes 802816 | tf_op jit(solution)/shard_map/dot_general | solution.py:69
  27.4 1.3 %fusion.19 = bf16[1,64,128]{2,1,0:T(8,128)(2,1)S(1)} fusion(bf16[64,2048]{1,0:T(8,128)(2,1)S(1)} %multiply_convert_fusion, bf16[2048,128]{1,0:T(8,128)(2,1)} %param.23), kind=kOutput, calls=%fused_computation.21 | convolution fusion | flops 33562624 | bytes 802816 | tf_op jit(solution)/shard_map/dot_general | solution.py:69
  28.7 0.0 copy-start.5
  28.7 1.3 %fusion.20 = bf16[1,64,128]{2,1,0:T(8,128)(2,1)S(1)} fusion(bf16[64,2048]{1,0:T(8,128)(2,1)S(1)} %multiply_convert_fusion, bf16[2048,128]{1,0:T(8,128)(2,1)} %param.24), kind=kOutput, calls=%fused_computation.22 | convolution fusion | flops 33562624 | bytes 802816 | tf_op jit(solution)/shard_map/dot_general | solution.py:69
  30.0 0.0 copy-start.2
  30.0 0.7 copy.66
  30.7 3.5 %all-to-all-start = ((bf16[4,64,128]{2,0,1:T(4,128)(2,1)}), bf16[4,64,128]{2,0,1:T(4,128)(2,1)S(1)}, u32[]{:S(2)}, u32[]{:S(2)}) async-start(bf16[4,64,128]{2,0,1:T(4,128)(2,1)} %copy.66), calls=%async_computation | async-start | bytes 131072 | tf_op jit(solution)/shard_map/all_to_all | solution.py:73
  34.2 0.7 log_bitcast_fusion
  34.9 0.8 convert_reduce_fusion.1
  35.7 5.3 %all-to-all-done = bf16[4,64,128]{2,0,1:T(4,128)(2,1)S(1)} async-done(((bf16[4,64,128]{2,0,1:T(4,128)(2,1)}), bf16[4,64,128]{2,0,1:T(4,128)(2,1)S(1)}, u32[]{:S(2)}, u32[]{:S(2)}) %all-to-all-start) | async-done | bytes 65568 | tf_op jit(solution)/shard_map/all_to_all | solution.py:73
  41.1 0.0 copy-start.3
  41.1 0.0 copy-start.6
  41.1 0.1 select_exponential_fusion
  41.2 4.4 %multiply_add_fusion = f32[4,16,128,128]{3,2,1,0:T(8,128)S(1)} fusion(f32[4,16,128,128]{3,2,1,0:T(8,128)} %param.17, f32[4,16,128]{2,1,0:T(8,128)S(1)} %fusion.57, f32[4,16,128]{2,1,0:T(8,128)S(1)} %get-tuple-element.3, f32[4,16,128]{2,1,0:T(8,128)S(1)} %get-tuple-element.2), kind=kLoop, calls=%fused_computation.6 | loop fusion | flops 3145728 | bytes 8486912 | tf_op jit(solution)/shard_map/add | solution.py:31
  45.6 0.0 copy-start.1
  45.6 2.0 %copy-done.1 = f32[4,16,128,128]{3,2,1,0:T(8,128)} copy-done((f32[4,16,128,128]{3,2,1,0:T(8,128)}, f32[4,16,128,128]{3,2,1,0:T(8,128)S(1)}, u32[]{:S(2)}) %copy-start.1) | copy-done | bytes 4194328
  47.6 3.6 %fusion.73 = f32[4,16,1,128]{3,2,1,0:T(1,128)S(1)} fusion(f32[4,16,128,1]{2,3,1,0:T(1,128)S(1)} %bitcast.137, f32[4,16,128,128]{3,2,1,0:T(8,128)S(1)} %multiply_add_fusion), kind=kOutput, calls=%fused_computation.103 | convolution fusion | flops 12582912 | bytes 4259840 | tf_op jit(solution)/shard_map/thk,thkv->thv/dot_general | solution.py:34
  51.3 0.1 multiply_reduce_fusion.2
  51.4 0.0 copy-done.5
  51.4 0.1 fusion.54
  51.5 18.4 %all-gather.1 = bf16[16,4,2048]{2,1,0:T(4,128)(2,1)S(1)} all-gather(bf16[1,4,2048]{2,1,0:T(4,128)(2,1)S(1)} %reshape.164), channel_id=1, replica_groups=mesh['grp'=2,'ep'=16] {'ep'}, dimensions={0}, use_global_device_ids=true | all-gather | bytes 278528 | tf_op jit(solution)/shard_map/all_gather | solution.py:76
  69.9 0.1 reshape.165
  70.0 0.0 copy-done.2
  70.0 0.8 convolution_convert_fusion.1
  70.8 3.5 %all-to-all-start.1 = ((bf16[16,4,128]{2,1,0:T(4,128)(2,1)}), bf16[16,4,128]{2,1,0:T(4,128)(2,1)S(1)}, u32[]{:S(2)}, u32[]{:S(2)}) async-start(bf16[16,4,128]{2,1,0:T(4,128)(2,1)} %bitcast.21), calls=%async_computation.1 | async-start | bytes 32768 | tf_op jit(solution)/shard_map/all_to_all | solution.py:78
  74.3 6.5 %all-to-all-done.1 = bf16[16,4,128]{2,1,0:T(4,128)(2,1)S(1)} async-done(((bf16[16,4,128]{2,1,0:T(4,128)(2,1)}), bf16[16,4,128]{2,1,0:T(4,128)(2,1)S(1)}, u32[]{:S(2)}, u32[]{:S(2)}) %all-to-all-start.1) | async-done | bytes 16416 | tf_op jit(solution)/shard_map/all_to_all | solution.py:78
  80.8 0.0 copy-done.3
  80.8 0.1 multiply_reduce_fusion.1
  80.9 0.0 copy-done.6
  80.9 0.2 convolution_convert_fusion
  81.2 0.1 broadcast_in_dim.2
  81.3 12.6 %all_to_all.38 = bf16[16,3,2048]{2,1,0:T(4,128)(2,1)S(1)} all-to-all(bf16[16,3,2048]{2,1,0:T(4,128)(2,1)S(1)} %bitcast.130), channel_id=1, replica_groups=mesh['grp'=2,'ep'=16] {'ep'}, dimensions={0} | all-to-all | bytes 393216 | tf_op jit(solution)/shard_map/all_to_all | solution.py:97
  93.9 4.5 %fusion.4 = f32[16,3,1792]{2,0,1:T(8,128)S(1)} fusion(bf16[2048,1792]{1,0:T(8,128)(2,1)} %param.29, bf16[16,3,2048]{2,1,0:T(4,128)(2,1)S(1)} %all_to_all.38), kind=kOutput, calls=%fused_computation.4 | convolution fusion | flops 352321536 | bytes 7880704 | tf_op jit(solution)/shard_map/scd,df->scf/dot_general | solution.py:98
  98.4 0.0 copy-start.7
  98.5 0.0 copy-start.4
  98.5 7.9 %fusion.12 = bf16[16,3,2048]{2,0,1:T(8,128)(2,1)S(1)} fusion(bf16[1792,2048]{1,0:T(8,128)(2,1)} %param.31, bf16[2048,1792]{1,0:T(8,128)(2,1)} %param.30, f32[16,3,1792]{2,0,1:T(8,128)S(1)} %fusion.4, bf16[16,3,2048]{2,1,0:T(4,128)(2,1)S(1)} %all_to_all.38), kind=kOutput, calls=%fused_computation.9 | convolution fusion | flops 705257472 | bytes 15417344 | tf_op jit(solution)/shard_map/scf,fd->scd/dot_general | solution.py:101
  106.4 0.9 copy.73
  107.2 3.5 %all-to-all-start.3 = ((bf16[16,3,2048]{2,1,0:T(4,128)(2,1)}), bf16[16,3,2048]{2,1,0:T(4,128)(2,1)S(1)}, u32[]{:S(2)}, u32[]{:S(2)}) async-start(bf16[16,3,2048]{2,1,0:T(4,128)(2,1)} %copy.73), calls=%async_computation.3 | async-start | bytes 524288 | tf_op jit(solution)/shard_map/all_to_all | solution.py:104
  110.8 0.0 copy-done.7
  110.8 0.0 copy-done.4
  110.8 0.1 fusion.63
  110.9 9.9 %all-to-all-done.3 = bf16[16,3,2048]{2,1,0:T(4,128)(2,1)S(1)} async-done(((bf16[16,3,2048]{2,1,0:T(4,128)(2,1)}), bf16[16,3,2048]{2,1,0:T(4,128)(2,1)S(1)}, u32[]{:S(2)}, u32[]{:S(2)}) %all-to-all-start.3) | async-done | bytes 196640 | tf_op jit(solution)/shard_map/all_to_all | solution.py:104
  120.7 0.1 convert_reduce_fusion
  120.9 0.9 fusion.16
  (13 shorter events, 0.2 us)
Async XLA Ops:
  0.6 25.2 %copy-start = (bf16[2048,128]{1,0:T(8,128)(2,1)S(1)}, bf16[2048,128]{1,0:T(8,128)(2,1)}, u32[]{:S(2)}) copy-start(bf16[2048,128]{1,0:T(8,128)(2,1)} %param.21) | copy-start | bytes 1572868
  28.7 22.7 %copy-start.5 = (f32[128]{0:T(128)S(1)}, f32[128]{0:T(128)}, u32[]{:S(2)}) copy-start(f32[128]{0:T(128)} %param.26) | copy-start | bytes 1540
  30.0 40.0 %copy-start.2 = (bf16[2048,128]{1,0:T(8,128)(2,1)S(1)}, bf16[2048,128]{1,0:T(8,128)(2,1)}, u32[]{:S(2)}) copy-start(bf16[2048,128]{1,0:T(8,128)(2,1)} %param.27) | copy-start | bytes 1572868
  30.7 10.4 %all-to-all-start = ((bf16[4,64,128]{2,0,1:T(4,128)(2,1)}), bf16[4,64,128]{2,0,1:T(4,128)(2,1)S(1)}, u32[]{:S(2)}, u32[]{:S(2)}) async-start(bf16[4,64,128]{2,0,1:T(4,128)(2,1)} %copy.66), calls=%async_computation | async-start | bytes 131072 | tf_op jit(solution)/shard_map/all_to_all | solution.py:73
  41.1 39.7 %copy-start.3 = (bf16[4,2048]{1,0:T(4,128)(2,1)S(1)}, bf16[4,2048]{1,0:T(4,128)(2,1)}, u32[]{:S(2)}) copy-start(bf16[4,2048]{1,0:T(4,128)(2,1)} %param.16) | copy-start | bytes 49156
  41.1 39.8 %copy-start.6 = (f32[2048]{0:T(1024)S(1)}, f32[2048]{0:T(1024)}, u32[]{:S(2)}) copy-start(f32[2048]{0:T(1024)} %param.28) | copy-start | bytes 24580
  45.6 2.0 %copy-start.1 = (f32[4,16,128,128]{3,2,1,0:T(8,128)}, f32[4,16,128,128]{3,2,1,0:T(8,128)S(1)}, u32[]{:S(2)}) copy-start(f32[4,16,128,128]{3,2,1,0:T(8,128)S(1)} %multiply_add_fusion) | copy-start | bytes 12582916
  70.8 10.0 %all-to-all-start.1 = ((bf16[16,4,128]{2,1,0:T(4,128)(2,1)}), bf16[16,4,128]{2,1,0:T(4,128)(2,1)S(1)}, u32[]{:S(2)}, u32[]{:S(2)}) async-start(bf16[16,4,128]{2,1,0:T(4,128)(2,1)} %bitcast.21), calls=%async_computation.1 | async-start | bytes 32768 | tf_op jit(solution)/shard_map/all_to_all | solution.py:78
  98.4 12.3 %copy-start.7 = (bf16[4,2]{0,1:T(2,128)(2,1)S(1)}, bf16[4,2]{0,1:T(2,128)(2,1)}, u32[]{:S(2)}) copy-start(bf16[4,2]{0,1:T(2,128)(2,1)} %param.19) | copy-start | bytes 52
  98.5 12.3 %copy-start.4 = (s32[4,2]{0,1:T(2,128)S(1)}, s32[4,2]{0,1:T(2,128)}, u32[]{:S(2)}) copy-start(s32[4,2]{0,1:T(2,128)} %param.18) | copy-start | bytes 100
  107.2 13.5 %all-to-all-start.3 = ((bf16[16,3,2048]{2,1,0:T(4,128)(2,1)}), bf16[16,3,2048]{2,1,0:T(4,128)(2,1)S(1)}, u32[]{:S(2)}, u32[]{:S(2)}) async-start(bf16[16,3,2048]{2,1,0:T(4,128)(2,1)} %copy.73), calls=%async_computation.3 | async-start | bytes 524288 | tf_op jit(solution)/shard_map/all_to_all | solution.py:104
where the time goes:
time: 123 us; the launch traced here: 122 us
  blocking collectives  55.2 us (45%)
  matrix products  22.1 us (18%)
  waiting for transfers between devices  21.7 us (18%)
  starting transfers between devices  10.5 us (9%)
  other arithmetic  7.51 us (6%)
  local copies, waits for them, and re-layouts  3.88 us (3%)
    all_gather x1, blocking collectives, local(): lax.all_gather(tokens, 'ep', axis=0, tiled=True)  24.2 us
    all_gather x1, blocking collectives, local(): lax.all_gather(mixed, 'ep', axis=0, tiled=True)  18.4 us
    all_to_all x1, blocking collectives, local(): lax.all_to_all(outgoing, 'ep', split_axis=0, concat_axis=0, tiled=True)  12.6 us
    all_to_all x1, waiting for transfers between devices, local(): lax.all_to_all(partial_rows.astype(jnp.bfloat16), 'ep', split_axis=0, con...  9.86 us
    dot_general x1, matrix products, local(): jnp.einsum('scf,fd->scd', hidden, expert_down, preferred_element_type=jnp...  7.88 us
    all_to_all x1, waiting for transfers between devices, local(): lax.all_to_all(mixer_cols, 'ep', split_axis=0, concat_axis=1, tiled=True)  6.45 us
    all_to_all x1, waiting for transfers between devices, local(): lax.all_to_all(projected, 'ep', split_axis=1, concat_axis=2, tiled=True)  5.34 us
    dot_general x1, matrix products, local(): jnp.einsum('scd,df->scf', arrived, expert_gate, preferred_element_type=jn...  4.49 us
  transfers between devices with their start and end apart: 3, of which 3 were waited for; matrix products, arithmetic and copies ran while one was open for 1% of the time, Pallas kernels for 0%

commit v1 on v0

--- a/solution.py
+++ b/solution.py
@@ -7,6 +7,14 @@
 EXPERTS = 4
 CAP = 3
 epsilon = 1e-06
+
+
+def order_the_column(load, on_dim):
+    num_devices = lax.axis_size("ep")
+    panels = tuple((num_devices if q == on_dim else 1 for q in range(load.ndim)))
+    a_next = jnp.tile(load, panels)
+    then = lax.all_to_all(a_next, axis_name="ep", split_axis=on_dim, concat_axis=on_dim, tiled=True)
+    return then
 
 
 def rms_scale(values, gain):
@@ -59,7 +67,7 @@
     model_width = tokens.shape[1]
     expert_group = FF // expert_gate.shape[1]
     all_tokens, all_ids, all_weights = (
-        lax.all_gather(tokens, "ep", axis=0, tiled=True),
+        order_the_column(tokens, 0),
         lax.all_gather(route_ids, "ep", axis=0, tiled=True),
         lax.all_gather(route_weights, "ep", axis=0, tiled=True),
     )

time: 123 us -> 118 us (0.959)
  blocking collectives: 55.2 us -> 31 us
  waiting for transfers between devices: 21.7 us -> 31.7 us
  starting transfers between devices: 10.5 us -> 17.9 us
  local copies, waits for them, and re-layouts: 3.88 us -> 5.55 us
    all_gather x1 -> x0, blocking collectives: 24.2 us -> none  [local(): lax.all_gather(tokens, 'ep', axis=0, tiled=True)]
    all_to_all x0 -> x1, waiting for transfers between devices: none -> 8.5 us  [order_the_column(): lax.all_to_all(a_next, axis_name='ep', split_axis=on_dim, concat_axis=on_...]
    all_to_all x0 -> x1, starting transfers between devices: none -> 7.41 us  [order_the_column(): lax.all_to_all(a_next, axis_name='ep', split_axis=on_dim, concat_axis=on_...]
    another operation x0 -> x1, local copies, waits for them, and re-layouts: none -> 1.58 us  [order_the_column(): a_next = jnp.tile(load, panels)]
    all_to_all x1, waiting for transfers between devices: 5.34 us -> 6.85 us  [local(): lax.all_to_all(projected, 'ep', split_axis=1, concat_axis=2, tiled=True)]
  transfers between devices with their start and end apart: 3 -> 4, of which waited for: 3 -> 4; matrix products, arithmetic and copies ran while one was open for 1% -> 1% of each run, Pallas kernels for 0% -> 0%
where the time goes in v1:
time: 118 us; the launch traced here: 117 us
  waiting for transfers between devices  31.7 us (27%)
  blocking collectives  31 us (26%)
  matrix products  22.1 us (19%)
  starting transfers between devices  17.9 us (15%)
  other arithmetic  7.58 us (6%)
  local copies, waits for them, and re-layouts  5.55 us (5%)
    all_gather x1, blocking collectives, local(): lax.all_gather(mixed, 'ep', axis=0, tiled=True)  18.4 us
    all_to_all x1, blocking collectives, local(): lax.all_to_all(outgoing, 'ep', split_axis=0, concat_axis=0, tiled=True)  12.6 us
    all_to_all x1, waiting for transfers between devices, local(): lax.all_to_all(partial_rows.astype(jnp.bfloat16), 'ep', split_axis=0, con...  9.86 us
    all_to_all x1, waiting for transfers between devices, order_the_column(): lax.all_to_all(a_next, axis_name='ep', split_axis=on_dim, concat_axis=on_...  8.5 us
    dot_general x1, matrix products, local(): jnp.einsum('scf,fd->scd', hidden, expert_down, preferred_element_type=jnp...  7.88 us
    all_to_all x1, starting transfers between devices, order_the_column(): lax.all_to_all(a_next, axis_name='ep', split_axis=on_dim, concat_axis=on_...  7.41 us
    all_to_all x1, waiting for transfers between devices, local(): lax.all_to_all(projected, 'ep', split_axis=1, concat_axis=2, tiled=True)  6.85 us
    all_to_all x1, waiting for transfers between devices, local(): lax.all_to_all(mixer_cols, 'ep', split_axis=0, concat_axis=1, tiled=True)  6.45 us
  transfers between devices with their start and end apart: 4, of which 4 were waited for; matrix products, arithmetic and copies ran while one was open for 1% of the time, Pallas kernels for 0%

profile of v1, /device:TPU:0, one launch (start us, length us, event | category | flops | bytes accessed | tf_op | source)
XLA Modules:
  0.0 116.8 jit_solution(5370064213257769578)
XLA Ops:
  0.6 0.0 copy-start
  0.6 1.6 %tile.2 = bf16[16,4,2048]{2,1,0:T(4,128)(2,1)} broadcast(bf16[4,2048]{1,0:T(4,128)(2,1)} %param.16), dimensions={1,2} | broadcast | bytes 278528 | tf_op jit(solution)/shard_map/tile | solution.py:15
  2.2 7.4 %all-to-all-start = ((bf16[16,4,2048]{2,1,0:T(4,128)(2,1)}), bf16[16,4,2048]{2,1,0:T(4,128)(2,1)S(1)}, u32[]{:S(2)}, u32[]{:S(2)}) async-start(bf16[16,4,2048]{2,1,0:T(4,128)(2,1)} %tile.2), calls=%async_computation | async-start | bytes 524288 | tf_op jit(solution)/shard_map/all_to_all | solution.py:16
  9.6 0.8 convert_reduce_fusion.1
  10.5 0.7 log_bitcast_fusion
  11.2 8.5 %all-to-all-done = bf16[16,4,2048]{2,1,0:T(4,128)(2,1)S(1)} async-done(((bf16[16,4,2048]{2,1,0:T(4,128)(2,1)}), bf16[16,4,2048]{2,1,0:T(4,128)(2,1)S(1)}, u32[]{:S(2)}, u32[]{:S(2)}) %all-to-all-start) | async-done | bytes 262176 | tf_op jit(solution)/shard_map/all_to_all | solution.py:16
  19.7 0.2 multiply_reduce_fusion
  19.9 0.1 rsqrt.28
  20.0 0.8 multiply_convert_fusion
  20.8 0.0 copy-done
  20.9 0.2 fusion.17
  21.1 1.3 %fusion.18 = bf16[1,64,128]{2,1,0:T(8,128)(2,1)S(1)} fusion(bf16[64,2048]{1,0:T(8,128)(2,1)S(1)} %multiply_convert_fusion, bf16[2048,128]{1,0:T(8,128)(2,1)} %param.22), kind=kOutput, calls=%fused_computation.20 | convolution fusion | flops 33562624 | bytes 802816 | tf_op jit(solution)/shard_map/dot_general | solution.py:77
  22.4 1.3 %fusion.19 = bf16[1,64,128]{2,1,0:T(8,128)(2,1)S(1)} fusion(bf16[64,2048]{1,0:T(8,128)(2,1)S(1)} %multiply_convert_fusion, bf16[2048,128]{1,0:T(8,128)(2,1)} %param.23), kind=kOutput, calls=%fused_computation.21 | convolution fusion | flops 33562624 | bytes 802816 | tf_op jit(solution)/shard_map/dot_general | solution.py:77
  23.7 0.0 copy-start.5
  23.7 1.3 %fusion.20 = bf16[1,64,128]{2,1,0:T(8,128)(2,1)S(1)} fusion(bf16[64,2048]{1,0:T(8,128)(2,1)S(1)} %multiply_convert_fusion, bf16[2048,128]{1,0:T(8,128)(2,1)} %param.24), kind=kOutput, calls=%fused_computation.22 | convolution fusion | flops 33562624 | bytes 802816 | tf_op jit(solution)/shard_map/dot_general | solution.py:77
  25.0 0.0 copy-start.2
  25.0 0.7 copy.91
  25.7 3.5 %all-to-all-start.1 = ((bf16[4,64,128]{2,0,1:T(4,128)(2,1)}), bf16[4,64,128]{2,0,1:T(4,128)(2,1)S(1)}, u32[]{:S(2)}, u32[]{:S(2)}) async-start(bf16[4,64,128]{2,0,1:T(4,128)(2,1)} %copy.91), calls=%async_computation.1 | async-start | bytes 131072 | tf_op jit(solution)/shard_map/all_to_all | solution.py:81
  29.2 6.8 %all-to-all-done.1 = bf16[4,64,128]{2,0,1:T(4,128)(2,1)S(1)} async-done(((bf16[4,64,128]{2,0,1:T(4,128)(2,1)}), bf16[4,64,128]{2,0,1:T(4,128)(2,1)S(1)}, u32[]{:S(2)}, u32[]{:S(2)}) %all-to-all-start.1) | async-done | bytes 65568 | tf_op jit(solution)/shard_map/all_to_all | solution.py:81
  36.1 0.0 copy-start.3
  36.1 0.0 copy-start.6
  36.1 0.1 select_exponential_fusion
  36.2 4.4 %multiply_add_fusion = f32[4,16,128,128]{3,2,1,0:T(8,128)S(1)} fusion(f32[4,16,128,128]{3,2,1,0:T(8,128)} %param.17, f32[4,16,128]{2,1,0:T(8,128)S(1)} %fusion.57, f32[4,16,128]{2,1,0:T(8,128)S(1)} %get-tuple-element.3, f32[4,16,128]{2,1,0:T(8,128)S(1)} %get-tuple-element.2), kind=kLoop, calls=%fused_computation.6 | loop fusion | flops 3145728 | bytes 8486912 | tf_op jit(solution)/shard_map/add | solution.py:39
  40.6 0.0 copy-start.1
  40.6 2.0 %copy-done.1 = f32[4,16,128,128]{3,2,1,0:T(8,128)} copy-done((f32[4,16,128,128]{3,2,1,0:T(8,128)}, f32[4,16,128,128]{3,2,1,0:T(8,128)S(1)}, u32[]{:S(2)}) %copy-start.1) | copy-done | bytes 4194328
  42.6 3.6 %fusion.73 = f32[4,16,1,128]{3,2,1,0:T(1,128)S(1)} fusion(f32[4,16,128,1]{2,3,1,0:T(1,128)S(1)} %bitcast.136, f32[4,16,128,128]{3,2,1,0:T(8,128)S(1)} %multiply_add_fusion), kind=kOutput, calls=%fused_computation.103 | convolution fusion | flops 12582912 | bytes 4259840 | tf_op jit(solution)/shard_map/thk,thkv->thv/dot_general | solution.py:42
  46.2 0.1 multiply_reduce_fusion.2
  46.4 0.0 copy-done.5
  46.4 0.1 fusion.54
  46.5 18.4 %all-gather = bf16[16,4,2048]{2,1,0:T(4,128)(2,1)S(1)} all-gather(bf16[1,4,2048]{2,1,0:T(4,128)(2,1)S(1)} %reshape.181), channel_id=1, replica_groups=mesh['grp'=2,'ep'=16] {'ep'}, dimensions={0}, use_global_device_ids=true | all-gather | bytes 278528 | tf_op jit(solution)/shard_map/all_gather | solution.py:84
  64.9 0.1 reshape.182
  64.9 0.0 copy-done.2
  65.0 0.8 convolution_convert_fusion.1
  65.8 3.5 %all-to-all-start.2 = ((bf16[16,4,128]{2,1,0:T(4,128)(2,1)}), bf16[16,4,128]{2,1,0:T(4,128)(2,1)S(1)}, u32[]{:S(2)}, u32[]{:S(2)}) async-start(bf16[16,4,128]{2,1,0:T(4,128)(2,1)} %bitcast.20), calls=%async_computation.2 | async-start | bytes 32768 | tf_op jit(solution)/shard_map/all_to_all | solution.py:86
  69.3 6.5 %all-to-all-done.2 = bf16[16,4,128]{2,1,0:T(4,128)(2,1)S(1)} async-done(((bf16[16,4,128]{2,1,0:T(4,128)(2,1)}), bf16[16,4,128]{2,1,0:T(4,128)(2,1)S(1)}, u32[]{:S(2)}, u32[]{:S(2)}) %all-to-all-start.2) | async-done | bytes 16416 | tf_op jit(solution)/shard_map/all_to_all | solution.py:86
  75.8 0.0 copy-done.3
  75.8 0.1 multiply_reduce_fusion.1
  75.9 0.0 copy-done.6
  75.9 0.2 convolution_convert_fusion
  76.2 0.1 broadcast_in_dim.2
  76.3 12.6 %all_to_all.44 = bf16[16,3,2048]{2,1,0:T(4,128)(2,1)S(1)} all-to-all(bf16[16,3,2048]{2,1,0:T(4,128)(2,1)S(1)} %bitcast.129), channel_id=1, replica_groups=mesh['grp'=2,'ep'=16] {'ep'}, dimensions={0} | all-to-all | bytes 393216 | tf_op jit(solution)/shard_map/all_to_all | solution.py:105
  88.9 4.5 %fusion.4 = f32[16,3,1792]{2,0,1:T(8,128)S(1)} fusion(bf16[2048,1792]{1,0:T(8,128)(2,1)} %param.29, bf16[16,3,2048]{2,1,0:T(4,128)(2,1)S(1)} %all_to_all.44), kind=kOutput, calls=%fused_computation.4 | convolution fusion | flops 352321536 | bytes 7880704 | tf_op jit(solution)/shard_map/scd,df->scf/dot_general | solution.py:106
  93.4 0.0 copy-start.7
  93.4 0.0 copy-start.4
  93.4 7.9 %fusion.12 = bf16[16,3,2048]{2,0,1:T(8,128)(2,1)S(1)} fusion(bf16[1792,2048]{1,0:T(8,128)(2,1)} %param.31, bf16[2048,1792]{1,0:T(8,128)(2,1)} %param.30, f32[16,3,1792]{2,0,1:T(8,128)S(1)} %fusion.4, bf16[16,3,2048]{2,1,0:T(4,128)(2,1)S(1)} %all_to_all.44), kind=kOutput, calls=%fused_computation.9 | convolution fusion | flops 705257472 | bytes 15417344 | tf_op jit(solution)/shard_map/scf,fd->scd/dot_general | solution.py:109
  101.3 0.9 copy.98
  102.2 3.5 %all-to-all-start.4 = ((bf16[16,3,2048]{2,1,0:T(4,128)(2,1)}), bf16[16,3,2048]{2,1,0:T(4,128)(2,1)S(1)}, u32[]{:S(2)}, u32[]{:S(2)}) async-start(bf16[16,3,2048]{2,1,0:T(4,128)(2,1)} %copy.98), calls=%async_computation.4 | async-start | bytes 524288 | tf_op jit(solution)/shard_map/all_to_all | solution.py:112
  105.7 0.0 copy-done.7
  105.8 0.0 copy-done.4
  105.8 0.1 fusion.63
  105.9 9.9 %all-to-all-done.4 = bf16[16,3,2048]{2,1,0:T(4,128)(2,1)S(1)} async-done(((bf16[16,3,2048]{2,1,0:T(4,128)(2,1)}), bf16[16,3,2048]{2,1,0:T(4,128)(2,1)S(1)}, u32[]{:S(2)}, u32[]{:S(2)}) %all-to-all-start.4) | async-done | bytes 196640 | tf_op jit(solution)/shard_map/all_to_all | solution.py:112
  115.7 0.1 convert_reduce_fusion
  115.8 0.9 fusion.16
  (13 shorter events, 0.2 us)
Async XLA Ops:
  0.6 20.2 %copy-start = (bf16[2048,128]{1,0:T(8,128)(2,1)S(1)}, bf16[2048,128]{1,0:T(8,128)(2,1)}, u32[]{:S(2)}) copy-start(bf16[2048,128]{1,0:T(8,128)(2,1)} %param.21) | copy-start | bytes 1572868
  2.2 17.4 %all-to-all-start = ((bf16[16,4,2048]{2,1,0:T(4,128)(2,1)}), bf16[16,4,2048]{2,1,0:T(4,128)(2,1)S(1)}, u32[]{:S(2)}, u32[]{:S(2)}) async-start(bf16[16,4,2048]{2,1,0:T(4,128)(2,1)} %tile.2), calls=%async_computation | async-start | bytes 524288 | tf_op jit(solution)/shard_map/all_to_all | solution.py:16
  23.7 22.7 %copy-start.5 = (f32[128]{0:T(128)S(1)}, f32[128]{0:T(128)}, u32[]{:S(2)}) copy-start(f32[128]{0:T(128)} %param.26) | copy-start | bytes 1540
  25.0 40.0 %copy-start.2 = (bf16[2048,128]{1,0:T(8,128)(2,1)S(1)}, bf16[2048,128]{1,0:T(8,128)(2,1)}, u32[]{:S(2)}) copy-start(bf16[2048,128]{1,0:T(8,128)(2,1)} %param.27) | copy-start | bytes 1572868
  25.7 10.4 %all-to-all-start.1 = ((bf16[4,64,128]{2,0,1:T(4,128)(2,1)}), bf16[4,64,128]{2,0,1:T(4,128)(2,1)S(1)}, u32[]{:S(2)}, u32[]{:S(2)}) async-start(bf16[4,64,128]{2,0,1:T(4,128)(2,1)} %copy.91), calls=%async_computation.1 | async-start | bytes 131072 | tf_op jit(solution)/shard_map/all_to_all | solution.py:81
  36.1 39.7 %copy-start.3 = (bf16[4,2048]{1,0:T(4,128)(2,1)S(1)}, bf16[4,2048]{1,0:T(4,128)(2,1)}, u32[]{:S(2)}) copy-start(bf16[4,2048]{1,0:T(4,128)(2,1)} %param.16) | copy-start | bytes 49156
  36.1 39.8 %copy-start.6 = (f32[2048]{0:T(1024)S(1)}, f32[2048]{0:T(1024)}, u32[]{:S(2)}) copy-start(f32[2048]{0:T(1024)} %param.28) | copy-start | bytes 24580
  40.6 2.0 %copy-start.1 = (f32[4,16,128,128]{3,2,1,0:T(8,128)}, f32[4,16,128,128]{3,2,1,0:T(8,128)S(1)}, u32[]{:S(2)}) copy-start(f32[4,16,128,128]{3,2,1,0:T(8,128)S(1)} %multiply_add_fusion) | copy-start | bytes 12582916
  65.8 10.0 %all-to-all-start.2 = ((bf16[16,4,128]{2,1,0:T(4,128)(2,1)}), bf16[16,4,128]{2,1,0:T(4,128)(2,1)S(1)}, u32[]{:S(2)}, u32[]{:S(2)}) async-start(bf16[16,4,128]{2,1,0:T(4,128)(2,1)} %bitcast.20), calls=%async_computation.2 | async-start | bytes 32768 | tf_op jit(solution)/shard_map/all_to_all | solution.py:86
  93.4 12.3 %copy-start.7 = (bf16[4,2]{0,1:T(2,128)(2,1)S(1)}, bf16[4,2]{0,1:T(2,128)(2,1)}, u32[]{:S(2)}) copy-start(bf16[4,2]{0,1:T(2,128)(2,1)} %param.19) | copy-start | bytes 52
  93.4 12.3 %copy-start.4 = (s32[4,2]{0,1:T(2,128)S(1)}, s32[4,2]{0,1:T(2,128)}, u32[]{:S(2)}) copy-start(s32[4,2]{0,1:T(2,128)} %param.18) | copy-start | bytes 100
  102.2 13.5 %all-to-all-start.4 = ((bf16[16,3,2048]{2,1,0:T(4,128)(2,1)}), bf16[16,3,2048]{2,1,0:T(4,128)(2,1)S(1)}, u32[]{:S(2)}, u32[]{:S(2)}) async-start(bf16[16,3,2048]{2,1,0:T(4,128)(2,1)} %copy.98), calls=%async_computation.4 | async-start | bytes 524288 | tf_op jit(solution)/shard_map/all_to_all | solution.py:112
